TPU v7x, 32 devices: a whole 2x2x4 slice. The times are simulated.
32 devices in a mesh: sp: 16 (over z, y, core), tp: 2 (over x).
Axes of the slice: x: 2, y: 2, z: 4, core: 2. Of those that a mesh axis runs over, the one named last changes fastest.
Arguments:
- incoming_activity: bfloat16 [8192, 2048], P(('sp', 'tp')), may hold values from -6 to 6
- entry_standardize_factor: bfloat16 [2048], replicated, may hold values from 0.099609375 to 1.8984375
- recursive_entry_matrix: bfloat16 [2048, 2048], P(None, 'tp'), may hold values from -0.125 to 0.125
- final_switch_matrix: bfloat16 [2048, 2048], P(None, 'tp'), may hold values from -0.125 to 0.125
- averaging_entry_matrix: bfloat16 [2048, 1024], P(None, 'tp'), may hold values from -0.125 to 0.125
- percolumn_filter_coefficients: bfloat16 [4, 2048], P(None, 'tp'), may hold values from -3 to 3
- switch_tiled_matrices: bfloat16 [2, 2, 32, 64, 64], P(None, None, 'tp'), may hold values from -0.75 to 0.75
- prior_fading_odds: float32 [2, 2048], P(None, 'tp'), may hold values from 2.7 to 17
- speed_factors: float32 [2, 8192], P(None, 'sp'), may hold values from 0.4 to 2.5, as said below
- extra_fading_amounts: float32 [2, 8192], P(None, 'sp'), may hold values from -1.39 to 0, as said below
- averaging_cluster_matrices: bfloat16 [8, 128, 128], P('tp'), may hold values from -0.5 to 0.5
- averaging_feature_factor: bfloat16 [1024], P('tp'), may hold values from 0.099609375 to 1.8984375
- recursive_final_matrix: bfloat16 [2048, 2048], P('tp'), may hold values from -0.25 to 0.25
- averaging_final_matrix: bfloat16 [1024, 2048], P('tp'), may hold values from -0.1875 to 0.1875
Outputs:
- mixed: bfloat16 [8192, 2048], P(('sp', 'tp'))
Inputs may be any that keep to these rules, and one draw needn't show every extreme that they name: `speed_factors`: constant over each aligned block of 512 positions. `extra_fading_amounts`: each row has at most two nonzero entries.
All inputs are finite; a program needn't handle non-finite values.
Results may differ from a plain program's by a relative error of at most 0.017.
Values may be sent and summed in bfloat16 or wider, within the bound.
A program may use at most 128 MiB of HBM per device.

v0:
```python
import jax
import jax.numpy as jnp
from jax import lax
from jax.sharding import PartitionSpec as P

FADING_FACTOR = 8.0
epsilon = 1e-06
span_rows = 16


def padded(block, sides, width):
    for axis, dim in sides:
        count = lax.axis_size(axis)
        forward = [(i, i + 1) for i in range(count - 1)]
        backward = [(target, source) for source, target in forward]
        low = lax.ppermute(
            lax.slice_in_dim(block, block.shape[dim] - width, None, axis=dim), axis, forward
        )
        high = lax.ppermute(lax.slice_in_dim(block, 0, width, axis=dim), axis, backward)
        block = jnp.concatenate([low, block, high], axis=dim)
    return block


def combine(earlier, later):
    return (earlier[0] * later[0], later[0] * earlier[1] + later[1])


def product(left, right):
    return jnp.dot(left, right, preferred_element_type=jnp.float32)


def block_chain(log_keep, drive, backward):
    length, width = log_keep.shape
    count = length // span_rows
    logs = log_keep.reshape(count, span_rows, width)
    sources = drive.reshape(count, span_rows, width)
    running = jnp.cumsum(logs, axis=1)
    place = jnp.arange(span_rows, dtype=jnp.int32)
    if backward:
        running = running[:, -1:] - running + logs
        inside = place[None, :] >= place[:, None]
    else:
        inside = place[None, :] <= place[:, None]
    inside = inside[None, :, :, None]
    spread = running[:, :, None, :] - running[:, None, :, :]
    weights = jnp.where(inside, jnp.exp(jnp.where(inside, spread, 0.0)), 0.0)
    within = jnp.einsum("btsc,bsc->btc", weights, sources)
    decay = jnp.exp(running)
    ones = jnp.ones((1, width), jnp.float32)
    zeros = jnp.zeros((1, width), jnp.float32)
    if backward:
        ends = (decay[:, 0], within[:, 0])
        total_keep, total_state = lax.associative_scan(combine, ends, axis=0, reverse=True)
        prior_keep = jnp.concatenate([total_keep[1:], ones], axis=0)
        prior_state = jnp.concatenate([total_state[1:], zeros], axis=0)
    else:
        ends = (decay[:, -1], within[:, -1])
        total_keep, total_state = lax.associative_scan(combine, ends, axis=0)
        prior_keep = jnp.concatenate([ones, total_keep[:-1]], axis=0)
        prior_state = jnp.concatenate([zeros, total_state[:-1]], axis=0)
    keep_all = decay * prior_keep[:, None]
    local_all = within + decay * prior_state[:, None]
    return (keep_all.reshape(length, width), local_all.reshape(length, width))


def local(
    incoming_activity,
    entry_standardize_factor,
    recursive_entry_matrix,
    final_switch_matrix,
    averaging_entry_matrix,
    percolumn_filter_coefficients,
    switch_tiled_matrices,
    prior_fading_odds,
    speed_factors,
    extra_fading_amounts,
    averaging_cluster_matrices,
    averaging_feature_factor,
    recursive_final_matrix,
    averaging_final_matrix,
):
    state_width = recursive_entry_matrix.shape[1]
    pool_width = averaging_entry_matrix.shape[1]
    gain = entry_standardize_factor.astype(jnp.float32)
    values = lax.all_gather(incoming_activity, "tp", axis=0, tiled=True).astype(jnp.float32)
    scaled = values * lax.rsqrt(jnp.mean(values * values, axis=1, keepdims=True) + epsilon)
    normed = (scaled * gain).astype(jnp.bfloat16)
    projected = jnp.concatenate(
        [
            product(normed, weight).astype(jnp.bfloat16)
            for weight in (recursive_entry_matrix, final_switch_matrix, averaging_entry_matrix)
        ],
        axis=1,
    )
    length = projected.shape[0]
    state_input = projected[:, :state_width]
    gate_input = projected[:, state_width : 2 * state_width]
    pool_input = projected[:, 2 * state_width :]
    conv_rows = padded(state_input, (("sp", 0),), 2).astype(jnp.float32)
    filtered = percolumn_filter_coefficients[0].astype(jnp.float32) * conv_rows[0:length]
    for shift in range(1, percolumn_filter_coefficients.shape[0]):
        filtered = (
            filtered
            + percolumn_filter_coefficients[shift].astype(jnp.float32)
            * conv_rows[shift : shift + length]
        )
    filtered = filtered.astype(jnp.bfloat16)
    filtered_wide = filtered.astype(jnp.float32)
    blocks_here = switch_tiled_matrices.shape[2]
    block_width = switch_tiled_matrices.shape[3]
    gate_sums = jnp.einsum(
        "tbi,dqbij->tdqbj",
        filtered.reshape(length, blocks_here, block_width),
        switch_tiled_matrices,
        preferred_element_type=jnp.float32,
    ).reshape(length, 2, 2, state_width)
    remember_switch = jax.nn.sigmoid(gate_sums[:, :, 0])
    inlet = jax.nn.sigmoid(gate_sums[:, :, 1])
    fading_speed = jax.nn.softplus(-prior_fading_odds)
    logarithmic_persistence = (
        -FADING_FACTOR
        * jnp.transpose(speed_factors)[:, :, None]
        * remember_switch
        * fading_speed[None]
        + jnp.transpose(extra_fading_amounts)[:, :, None]
    )
    drive = jnp.sqrt(-jnp.expm1(2.0 * logarithmic_persistence)) * inlet * filtered_wide[:, None, :]
    forward_keep, forward_local = block_chain(logarithmic_persistence[:, 0], drive[:, 0], False)
    backward_keep, backward_local = block_chain(logarithmic_persistence[:, 1], drive[:, 1], True)
    zeros = jnp.zeros((state_width,), jnp.float32)
    summary = jnp.stack([forward_keep[-1], forward_local[-1], backward_keep[0], backward_local[0]])[
        None
    ]
    totals = lax.all_gather(summary, "sp", axis=0, tiled=True)
    place = lax.axis_index("sp")
    forward_all = lax.associative_scan(combine, (totals[:, 0], totals[:, 1]), axis=0)
    backward_all = lax.associative_scan(combine, (totals[:, 2], totals[:, 3]), axis=0, reverse=True)
    forward_before = jnp.concatenate([zeros[None], forward_all[1]], axis=0)
    backward_after = jnp.concatenate([backward_all[1], zeros[None]], axis=0)
    forward_carry = lax.dynamic_index_in_dim(forward_before, place, 0, keepdims=False)
    backward_carry = lax.dynamic_index_in_dim(backward_after, place + 1, 0, keepdims=False)
    state_sum = (
        forward_local
        + forward_keep * forward_carry[None]
        + backward_local
        + backward_keep * backward_carry[None]
    )
    state_mix = (jax.nn.gelu(gate_input.astype(jnp.float32)) * state_sum).astype(jnp.bfloat16)
    pool_rows = padded(pool_input, (("sp", 0),), 8).astype(jnp.float32)
    spans = []
    level = pool_rows
    for step in range(4):
        shift = 1 << step
        level = level[:-shift] + level[shift:]
        spans.append(level)
    group_width = averaging_cluster_matrices.shape[1]
    local_groups = pool_width // group_width
    group_index = (
        lax.axis_index("tp") * local_groups + jnp.arange(pool_width, dtype=jnp.int32) // group_width
    )
    window_code = group_index % 4
    position = lax.axis_index("sp") * length + jnp.arange(length, dtype=jnp.int32)
    total_length = length * lax.axis_size("sp")
    window_sum = jnp.zeros((length, pool_width), jnp.float32)
    counted = jnp.ones((length, pool_width), jnp.float32)
    for code in range(4):
        half = 1 << code
        begin = 8 - half
        chosen = (window_code == code)[None, :]
        window_count = (
            jnp.minimum(position + half, total_length) - jnp.maximum(position - half, 0)
        ).astype(jnp.float32)[:, None]
        window_sum = jnp.where(chosen, spans[code][begin : begin + length], window_sum)
        counted = jnp.where(chosen, window_count, counted)
    pooled = (window_sum / counted - pool_rows[8 : 8 + length]).astype(jnp.bfloat16)
    grouped = jnp.einsum(
        "tgi,gij->tgj",
        pooled.reshape(length, local_groups, group_width),
        averaging_cluster_matrices,
        preferred_element_type=jnp.float32,
    ).reshape(length, pool_width)
    pool_mix = (grouped * averaging_feature_factor.astype(jnp.float32)).astype(jnp.bfloat16)
    return lax.psum_scatter(
        (
            product(state_mix, recursive_final_matrix) + product(pool_mix, averaging_final_matrix)
        ).astype(jnp.bfloat16),
        "tp",
        scatter_dimension=0,
        tiled=True,
    )


def solution(mesh):
    in_specs = (
        P(("sp", "tp"), None),
        P(),
        P(None, "tp"),
        P(None, "tp"),
        P(None, "tp"),
        P(None, "tp"),
        P(None, None, "tp", None, None),
        P(None, "tp"),
        P(None, "sp"),
        P(None, "sp"),
        P("tp", None, None),
        P("tp"),
        P("tp", None),
        P("tp", None),
    )
    out_specs = P(("sp", "tp"), None)
    return jax.shard_map(local, mesh=mesh, in_specs=in_specs, out_specs=out_specs, check_vma=False)
```

profile of v0, /device:TPU:0, one launch (start us, length us, event | category | flops | bytes accessed | tf_op | source)
XLA Modules:
  0.0 251.2 jit_solution(8073936475268317214)
XLA Ops:
  8.7 1.6 copy.54
  10.5 34.2 %all-gather.4.cloned.1.call-done = bf16[512,2048]{1,0:T(8,128)(2,1)} async-done(((bf16[256,2048]{1,0:T(8,128)(2,1)}), bf16[512,2048]{1,0:T(8,128)(2,1)}) %all-gather.4.cloned.1.call-update) | async-done | bytes 2097168 | tf_op jit(solution)/shard_map/all_gather | solution.py:85
  44.7 2.2 fusion
  47.0 4.7 %convolution_convert_fusion = bf16[512,1024]{1,0:T(8,128)(2,1)S(1)} fusion(bf16[2048,1024]{1,0:T(8,128)(2,1)} %param.16, bf16[512,2048]{1,0:T(8,128)(2,1)S(1)} %copy-done.9, f32[2048]{0:T(1024)S(1)} %convert_element_type.85, f32[512]{0:T(512)S(1)} %add_rsqrt_fusion), kind=kOutput, calls=%fused_computation.44 | convolution fusion | flops 2152202240 | bytes 7350272 | tf_op jit(solution)/shard_map/dot_general | solution.py:29
  51.8 1.6 collective-permute-start
  56.0 4.5 %collective-permute-start.2 = (bf16[8,512]{1,0:T(8,128)(2,1)S(1)}, bf16[8,512]{1,0:T(8,128)(2,1)S(1)}, u32[]{:S(2)}, u32[]{:S(2)}) collective-permute-start(bf16[8,512]{1,0:T(8,128)(2,1)S(1)} %get-tuple-element.24), channel_id=1, source_target_pairs={{0,2},{2,4},{4,6},{6,8},{8,10},{10,12},{12,14},{14,16},{16,18},{18... | collective-permute-start | bytes 24584 | tf_op jit(solution)/shard_map/ppermute | solution.py:16
  62.1 2.6 %fusion.71 = (f32[512,1024]{1,0:T(8,128)}, bf16[512,1024]{1,0:T(8,128)(2,1)}) fusion(f32[516,1024]{1,0:T(8,128)S(1)} %maximum_convert_fusion, f32[1024]{0:T(1024)S(1)} %bitcast.154, f32[1024]{0:T(1024)S(1)} %bitcast.155, f32[1024]{0:T(1024)S(1)} %bitcast.153, f32[1024]{0:T(1024)S(1)} %bitcast.152), kind=kLoop, calls=%fused_computation.227 | loop fusion | flops 4718592 | bytes 11550720 | tf_op jit(solution)/shard_map/convert_element_type | solution.py:108
  64.7 2.8 %copy.53 = bf16[512,1024]{0,1:T(8,128)(2,1)} copy(bf16[512,1024]{1,0:T(8,128)(2,1)} %get-tuple-element.8) | data formatting | bytes 2097152 | tf_op jit(solution)/shard_map/convert_element_type | solution.py:107
  67.4 2.5 fusion.96
  69.9 1.8 copy.55
  71.7 4.2 %fusion.74 = (f32[512,2,1,1024]{0,3,2,1:T(8,128)}, f32[512,2,1,1024]{0,3,2,1:T(8,128)}) fusion(f32[512,2,2,1024]{0,3,2,1:T(8,128)S(1)} %bitcast.122), kind=kLoop, calls=%fused_computation.229 | loop fusion | bytes 16777216 | tf_op jit(solution)/shard_map/slice | solution.py:117
  75.9 5.4 %copy.92 = f32[512,2,1,1024]{3,0,1,2:T(8,128)} copy(f32[512,2,1,1024]{0,3,2,1:T(8,128)} %get-tuple-element.12) | data formatting | bytes 8388608
  81.3 5.4 %copy.93 = f32[512,2,1,1024]{3,0,1,2:T(8,128)} copy(f32[512,2,1,1024]{0,3,2,1:T(8,128)} %get-tuple-element.13) | data formatting | bytes 8388608
  86.7 7.3 %fusion.3 = (f32[512,2,1024]{2,0,1:T(8,128)S(1)}, f32[512,2,1024]{2,0,1:T(8,128)S(1)}) fusion(f32[512,2,1,1024]{3,0,1,2:T(8,128)} %copy.93, f32[512,1024]{1,0:T(8,128)} %get-tuple-element.7, f32[512,2]{0,1:T(2,128)S(1)} %bitcast.158, f32[2,1024]{1,0:T(2,128)S(1)} %compare_select_fusion, f32[512,2,1,1024]{3,0,1,2:T(8,128)} %copy.92, ...), kind=kLoop, calls=%fused_computation.8 | loop fusion | flops 13631488 | bytes 18890752 | tf_op jit(solution)/shard_map/mul | solution.py:127
  94.0 3.3 %fusion.75 = (f32[512,1,1024]{2,0,1:T(8,128)}, f32[512,1,1024]{2,0,1:T(8,128)S(1)}, f32[512,1,1024]{2,0,1:T(8,128)}, f32[512,1,1024]{2,0,1:T(8,128)}) fusion(f32[512,2,1024]{2,0,1:T(8,128)S(1)} %get-tuple-element.6, f32[512,2,1024]{2,0,1:T(8,128)S(1)} %get-tuple-element.5), kind=kLoop, calls=%fused_computation.230 | loop fusion | bytes 16777216 | tf_op jit(solution)/shard_map/slice | solution.py:128
  99.2 3.6 %fusion.73 = (f32[32,16,1024]{2,0,1:T(8,128)S(1)}, f32[32,16,1024]{2,0,1:T(8,128)}, f32[32,16,1024]{2,0,1:T(8,128)}) fusion(f32[32,16,1024]{2,1,0:T(8,128)S(1)} %bitcast.124, f32[32,16,1024]{2,0,1:T(8,128)S(1)} %fusion.20, f32[32,1024]{1,0:T(8,128)S(1)} %slice_bitcast_fusion.2), kind=kLoop, calls=%fused_computation.228 | loop fusion | flops 1048576 | bytes 10616832 | tf_op jit(solution)/shard_map/exp | solution.py:48
  102.9 3.0 %copy.66 = f32[32,16,1024]{2,1,0:T(8,128)S(1)} copy(f32[32,16,1024]{2,0,1:T(8,128)} %get-tuple-element.10) | data formatting | bytes 4194304 | tf_op jit(solution)/shard_map/add | solution.py:40
  105.9 12.3 %multiply_reduce_fusion = f32[32,1024,16]{1,2,0:T(8,128)S(1)} fusion(f32[32,1024,16]{1,2,0:T(8,128)S(1)} %bitcast.139, f32[32,16,1024]{2,1,0:T(8,128)S(1)} %copy.66, pred[16,16]{1,0:T(8,128)(4,1)S(1)} %iota_compare_fusion), kind=kLoop, calls=%fused_computation | loop fusion | flops 41418752 | bytes 6291712
  120.9 4.3 %fusion.95 = (f32[32,16,1024]{2,0,1:T(8,128)S(1)}, f32[32,16,1024]{2,0,1:T(8,128)}) fusion(f32[32,16,1024]{2,1,0:T(8,128)} %bitcast.125), kind=kOutput, calls=%fused_computation.250 | output fusion | flops 7864320 | bytes 6291456 | tf_op jit(solution)/shard_map/jit(cumsum)/reduce_window_sum | solution.py:37
  125.3 3.0 %copy.59 = f32[32,16,1024]{2,1,0:T(8,128)S(1)} copy(f32[32,16,1024]{2,0,1:T(8,128)} %get-tuple-element.97) | data formatting | bytes 4194304 | tf_op jit(solution)/shard_map/jit(cumsum)/reduce_window_sum | solution.py:37
  128.3 12.1 %multiply_reduce_fusion.1 = f32[32,1024,16]{1,2,0:T(8,128)S(1)} fusion(f32[32,1024,16]{1,2,0:T(8,128)S(1)} %bitcast.138, f32[32,16,1024]{2,1,0:T(8,128)S(1)} %copy.59, pred[16,16]{1,0:T(8,128)(4,1)S(1)} %iota_compare_fusion.1), kind=kLoop, calls=%fused_computation.1 | loop fusion | flops 41418752 | bytes 6291712
  142.5 4.1 %copy.64 = f32[32,16,1024]{2,1,0:T(8,128)} copy(f32[32,16,1024]{2,0,1:T(8,128)} %get-tuple-element.11) | data formatting | bytes 4194304 | tf_op jit(solution)/shard_map/sub | solution.py:40
  148.2 3.7 %multiply_add_fusion = f32[32,16,1024]{2,0,1:T(8,128)S(1)} fusion(f32[32,1024]{1,0:T(8,128)S(1)} %concatenate.110, f32[32,1024,16]{1,2,0:T(8,128)} %copy-done.3, f32[32,16,1024]{2,0,1:T(8,128)} %get-tuple-element.10), kind=kLoop, calls=%fused_computation.39 | loop fusion | flops 1048576 | bytes 6422528 | tf_op jit(solution)/shard_map/add | solution.py:62
  153.2 1.4 copy-done.6
  154.9 2.8 %bitcast_multiply_fusion.2 = f32[512,1024]{1,0:T(8,128)S(1)} fusion(f32[32,16,1024]{2,1,0:T(8,128)} %copy.64, f32[32,1024]{1,0:T(8,128)S(1)} %concatenate.105, f32[512,2,1024]{2,0,1:T(8,128)} %copy-done.1), kind=kLoop, calls=%fused_computation.32 | loop fusion | flops 1048576 | bytes 6422528 | tf_op jit(solution)/shard_map/mul | solution.py:61
  157.7 1.4 copy-done.5
  159.9 3.7 %broadcast_multiply_fusion = (f32[32,16,1024]{2,0,1:T(8,128)S(1)}, f32[32,16,1024]{2,0,1:T(8,128)S(1)}) fusion(f32[32,1024]{1,0:T(8,128)S(1)} %concatenate.100, f32[32,16,1024]{2,0,1:T(8,128)} %get-tuple-element.97, f32[32,1024]{1,0:T(8,128)S(1)} %concatenate.95, f32[32,1024,16]{1,2,0:T(8,128)} %copy-done.4), kind=kLoop, calls=%fused_computation.62 | loop fusion | flops 1572864 | bytes 8650752 | tf_op jit(solution)/shard_map/mul | solution.py:61
  166.2 1.4 copy-done.8
  167.6 24.5 %all-gather.1 = f32[16,4,1024]{2,1,0:T(4,128)S(1)} all-gather(f32[1,4,1024]{2,1,0:T(4,128)S(1)} %maximum_bitcast_fusion), channel_id=2, replica_groups=mesh['sp'=16,'tp'=2] {'sp'}, dimensions={0}, use_global_device_ids=true | all-gather | bytes 278528 | tf_op jit(solution)/shard_map/all_gather | solution.py:134
  195.6 13.8 %fusion.28 = f32[512,2048]{1,0:T(8,128)} fusion(bf16[1024,2048]{1,0:T(8,128)(2,1)} %param.26, f32[512,1024]{1,0:T(8,128)} %copy-done.5, f32[512,1024]{1,0:T(8,128)} %bitcast.133, f32[512,1024]{1,0:T(8,128)} %bitcast.137, f32[512,1024]{1,0:T(8,128)} %bitcast.135, bf16[2048,1024]{1,0:T(8,128)(2,1)} %param.17, f32[1024]{0:T(1024)S(1)} %bitcast.157, ...), kind=kOutput, calls=%fused_computation.63 | convolution fusion | flops 4308074496 | bytes 23087104 | tf_op jit(solution)/shard_map/dot_general | solution.py:29
  213.1 2.6 %add_convert_fusion = bf16[512,2048]{1,0:T(8,128)(2,1)} fusion(f32[512,2048]{1,0:T(8,128)S(1)} %copy-done.2, bf16[512,512]{0,1:T(8,128)(2,1)S(1)} %fusion.27, bf16[512,2048]{1,0:T(8,128)(2,1)S(1)} %copy-done), kind=kOutput, calls=%fused_computation.12 | convolution fusion | flops 1075838976 | bytes 8912896 | tf_op jit(solution)/shard_map/dot_general | solution.py:29
  215.7 28.4 %reduce-scatter.2.cloned.1.call-done = bf16[256,2048]{1,0:T(8,128)(2,1)} async-done(((bf16[512,2048]{1,0:T(8,128)(2,1)}), bf16[256,2048]{1,0:T(8,128)(2,1)}) %reduce-scatter.2.cloned.1.call-update) | async-done | bytes 1048592 | tf_op jit(solution)/shard_map/reduce_scatter | solution.py:183
  (329 shorter events, 25.7 us)
Async XLA Ops:
  6.5 205.8 %copy-start = (bf16[512,2048]{1,0:T(8,128)(2,1)S(1)}, bf16[512,2048]{1,0:T(8,128)(2,1)}, u32[]{:S(2)}) copy-start(bf16[512,2048]{1,0:T(8,128)(2,1)} %param.27) | copy-start | bytes 6291460
  6.5 3.9 %copy-start.16 = (f32[2,512]{1,0:T(2,128)S(1)}, f32[2,512]{1,0:T(2,128)}, u32[]{:S(2)}) copy-start(f32[2,512]{1,0:T(2,128)} %param.22) | copy-start | bytes 12292
  6.5 3.9 %copy-start.15 = (f32[2,1024]{1,0:T(2,128)S(1)}, f32[2,1024]{1,0:T(2,128)}, u32[]{:S(2)}) copy-start(f32[2,1024]{1,0:T(2,128)} %param.21) | copy-start | bytes 24580
  6.5 3.9 %copy-start.14 = (bf16[4,1024]{1,0:T(4,128)(2,1)S(1)}, bf16[4,1024]{1,0:T(4,128)(2,1)}, u32[]{:S(2)}) copy-start(bf16[4,1024]{1,0:T(4,128)(2,1)} %param.19) | copy-start | bytes 24580
  6.5 38.2 %all-gather.4.cloned.1.call-start = ((), (), s32[]{:S(2)}) async-start(), calls=%async_computation.1 | async-start | bytes 3145728 | tf_op jit(solution)/shard_map/all_gather | solution.py:85
  7.3 236.9 %reduce-scatter.2.cloned.1.call-start = ((), (), s32[]{:S(2)}) async-start(), calls=%async_computation.2 | async-start | bytes 3145728 | tf_op jit(solution)/shard_map/reduce_scatter | solution.py:183
  44.7 2.2 copy-start.9
  47.0 7.6 %copy-start.18 = (bf16[2048,512]{1,0:T(8,128)(2,1)S(1)}, bf16[2048,512]{1,0:T(8,128)(2,1)}, u32[]{:S(2)}) copy-start(bf16[2048,512]{1,0:T(8,128)(2,1)} %param.18) | copy-start | bytes 6291460
  51.8 10.0 %collective-permute-start = (bf16[2,1024]{1,0:T(2,128)(2,1)S(1)}, bf16[2,1024]{1,0:T(2,128)(2,1)S(1)}, u32[]{:S(2)}, u32[]{:S(2)}) collective-permute-start(bf16[2,1024]{1,0:T(2,128)(2,1)S(1)} %get-tuple-element.22), channel_id=1, source_target_pairs={{0,2},{2,4},{4,6},{6,8},{8,10},{10,12},{12,14},{14,16},{16,18},{18... | collective-permute-start | bytes 12296 | tf_op jit(solution)/shard_map/ppermute | solution.py:16
  53.3 8.4 %collective-permute-start.1 = (bf16[2,1024]{1,0:T(2,128)(2,1)S(1)}, bf16[2,1024]{1,0:T(2,128)(2,1)S(1)}, u32[]{:S(2)}, u32[]{:S(2)}) collective-permute-start(bf16[2,1024]{1,0:T(2,128)(2,1)S(1)} %get-tuple-element.23), channel_id=1, source_target_pairs={{2,0},{4,2},{6,4},{8,6},{10,8},{12,10},{14,12},{16,14},{18,16},{20... | collective-permute-start | bytes 12296 | tf_op jit(solution)/shard_map/ppermute | solution.py:19
  55.9 6.1 %copy-start.12 = (bf16[512,512]{1,0:T(8,128)(2,1)}, bf16[512,512]{1,0:T(8,128)(2,1)S(1)}, u32[]{:S(2)}) copy-start(bf16[512,512]{1,0:T(8,128)(2,1)S(1)} %convolution_convert_fusion.2) | copy-start | bytes 1572868
  56.0 153.4 %collective-permute-start.2 = (bf16[8,512]{1,0:T(8,128)(2,1)S(1)}, bf16[8,512]{1,0:T(8,128)(2,1)S(1)}, u32[]{:S(2)}, u32[]{:S(2)}) collective-permute-start(bf16[8,512]{1,0:T(8,128)(2,1)S(1)} %get-tuple-element.24), channel_id=1, source_target_pairs={{0,2},{2,4},{4,6},{6,8},{8,10},{10,12},{12,14},{14,16},{16,18},{18... | collective-permute-start | bytes 24584 | tf_op jit(solution)/shard_map/ppermute | solution.py:16
  60.4 148.9 %collective-permute-start.3 = (bf16[8,512]{1,0:T(8,128)(2,1)S(1)}, bf16[8,512]{1,0:T(8,128)(2,1)S(1)}, u32[]{:S(2)}, u32[]{:S(2)}) collective-permute-start(bf16[8,512]{1,0:T(8,128)(2,1)S(1)} %get-tuple-element.25), channel_id=1, source_target_pairs={{2,0},{4,2},{6,4},{8,6},{10,8},{12,10},{14,12},{16,14},{18,16},{20... | collective-permute-start | bytes 24584 | tf_op jit(solution)/shard_map/ppermute | solution.py:19
  81.3 5.4 %copy-start.17 = (f32[2,512]{1,0:T(2,128)S(1)}, f32[2,512]{1,0:T(2,128)}, u32[]{:S(2)}) copy-start(f32[2,512]{1,0:T(2,128)} %param.23) | copy-start | bytes 12292
  94.0 3.9 %copy-start.1 = (f32[512,2,1024]{2,0,1:T(8,128)}, f32[512,2,1024]{2,0,1:T(8,128)S(1)}, u32[]{:S(2)}) copy-start(f32[512,2,1024]{2,0,1:T(8,128)S(1)} %get-tuple-element.6) | copy-start | bytes 12582916
  102.9 3.0 %copy-start.11 = (f32[512,1,1024]{2,0,1:T(8,128)S(1)}, f32[512,1,1024]{2,0,1:T(8,128)}, u32[]{:S(2)}) copy-start(f32[512,1,1024]{2,0,1:T(8,128)} %get-tuple-element.98) | copy-start | bytes 6291460
  118.2 1.3 copy-start.3
  125.3 3.0 %copy-start.10 = (f32[512,1,1024]{2,0,1:T(8,128)S(1)}, f32[512,1,1024]{2,0,1:T(8,128)}, u32[]{:S(2)}) copy-start(f32[512,1,1024]{2,0,1:T(8,128)} %get-tuple-element.99) | copy-start | bytes 6291460
  140.4 1.3 copy-start.4
  153.2 1.4 copy-start.6
  157.7 1.4 copy-start.5
  164.9 1.3 copy-start.7
  166.2 1.4 copy-start.8
  195.6 13.8 %copy-start.13 = (bf16[512,512]{1,0:T(8,128)(2,1)S(1)}, bf16[512,512]{1,0:T(8,128)(2,1)}, u32[]{:S(2)}) copy-start(bf16[512,512]{1,0:T(8,128)(2,1)} %copy-done.12) | copy-start | bytes 1572868
  210.0 0.9 copy-start.19
  210.9 2.2 copy-start.2
Sparse Core Ops, SparseCore 0:
  8.9 35.8 all-gather.3
  215.9 28.2 reduce-scatter.1
where the time goes:
time: 256 us; the launch traced here: 251 us
  waiting for transfers between devices  63.3 us (25%)
  other arithmetic  59.5 us (23%)
  local copies, waits for them, and re-layouts  53.5 us (21%)
  matrix products  26.1 us (10%)
  blocking collectives  24.5 us (10%)
  between operations  15.5 us (6%)
  starting transfers between devices  8.69 us (3%)
    all_gather x1, waiting for transfers between devices, local(): lax.all_gather(incoming_activity, 'tp', axis=0, tiled=True)  34.2 us
    reduce_scatter x1, waiting for transfers between devices, local(): lax.psum_scatter((product(state_mix, recursive_final_matrix) + product(po...  28.4 us
    all_gather x1, blocking collectives, local(): totals = lax.all_gather(summary, 'sp', axis=0, tiled=True)  24.5 us
    unnamed x3, other arithmetic  24.5 us
    dot_general x4, matrix products, product(): return jnp.dot(left, right, preferred_element_type=jnp.float32)  22.4 us
    unnamed x51, local copies, waits for them, and re-layouts  18.9 us
    mul x1, other arithmetic, local(): jnp.sqrt(-jnp.expm1(2.0 * logarithmic_persistence)) * inlet  7.26 us
    mul x2, other arithmetic, block_chain(): keep_all = decay * prior_keep[:, None]  6.51 us
  transfers between devices with their start and end apart: 6, of which 2 were waited for; matrix products, arithmetic and copies ran while one was open for 48% of the time, Pallas kernels for 0%

commit v1 on v0

--- a/solution.py
+++ b/solution.py
@@ -131,7 +131,14 @@
     summary = jnp.stack([forward_keep[-1], forward_local[-1], backward_keep[0], backward_local[0]])[
         None
     ]
-    totals = lax.all_gather(summary, "sp", axis=0, tiled=True)
+    ways, here = (lax.axis_size("sp"), lax.axis_index("sp"))
+    totals, reach = (summary, 1)
+    while reach < ways:
+        theirs = lax.ppermute(totals, "sp", [(d, d ^ reach) for d in range(ways)])
+        mine_first = jnp.concatenate([totals, theirs], axis=0)
+        theirs_first = jnp.concatenate([theirs, totals], axis=0)
+        totals = jnp.where(here & reach == 0, mine_first, theirs_first)
+        reach = 2 * reach
     place = lax.axis_index("sp")
     forward_all = lax.associative_scan(combine, (totals[:, 0], totals[:, 1]), axis=0)
     backward_all = lax.associative_scan(combine, (totals[:, 2], totals[:, 3]), axis=0, reverse=True)

time: 256 us -> 253 us (0.988)
  blocking collectives: 24.5 us -> 0 us
  starting transfers between devices: 8.69 us -> 20.1 us
  waiting for transfers between devices: 63.3 us -> 73.9 us
  local copies, waits for them, and re-layouts: 53.5 us -> 50.8 us
    all_gather x1 -> x0, blocking collectives: 24.5 us -> none  [local(): totals = lax.all_gather(summary, 'sp', axis=0, tiled=True)]
    ppermute x0 -> x4, starting transfers between devices: none -> 11.4 us  [local(): theirs = lax.ppermute(totals, 'sp', [(d, d ^ reach) for d in range(ways)])]
    ppermute x0 -> x4, waiting for transfers between devices: none -> 5.96 us  [local(): theirs = lax.ppermute(totals, 'sp', [(d, d ^ reach) for d in range(ways)])]
    reduce_scatter x1, waiting for transfers between devices: 28.4 us -> 33 us  [local(): lax.psum_scatter((product(state_mix, recursive_final_matrix) + product(po...]
    unnamed x51 -> x49, local copies, waits for them, and re-layouts: 18.9 us -> 16.2 us
    unnamed x3 -> x2, other arithmetic: 24.5 us -> 24.4 us
  transfers between devices with their start and end apart: 6 -> 10, of which waited for: 2 -> 6; matrix products, arithmetic and copies ran while one was open for 48% -> 43% of each run, Pallas kernels for 0% -> 0%
where the time goes in v1:
time: 253 us; the launch traced here: 248 us
  waiting for transfers between devices  73.9 us (29%)
  other arithmetic  59.6 us (24%)
  local copies, waits for them, and re-layouts  50.8 us (20%)
  matrix products  28.3 us (11%)
  starting transfers between devices  20.1 us (8%)
  between operations  15.5 us (6%)
    all_gather x1, waiting for transfers between devices, local(): lax.all_gather(incoming_activity, 'tp', axis=0, tiled=True)  34.2 us
    reduce_scatter x1, waiting for transfers between devices, local(): lax.psum_scatter((product(state_mix, recursive_final_matrix) + product(po...  33 us
    dot_general x4, matrix products, product(): return jnp.dot(left, right, preferred_element_type=jnp.float32)  24.6 us
    unnamed x2, other arithmetic  24.4 us
    unnamed x49, local copies, waits for them, and re-layouts  16.2 us
    ppermute x4, starting transfers between devices, local(): theirs = lax.ppermute(totals, 'sp', [(d, d ^ reach) for d in range(ways)])  11.4 us
    mul x1, other arithmetic, local(): jnp.sqrt(-jnp.expm1(2.0 * logarithmic_persistence)) * inlet  7.26 us
    mul x2, other arithmetic, block_chain(): keep_all = decay * prior_keep[:, None]  6.51 us
  transfers between devices with their start and end apart: 10, of which 6 were waited for; matrix products, arithmetic and copies ran while one was open for 43% of the time, Pallas kernels for 0%

profile of v1, /device:TPU:0, one launch (start us, length us, event | category | flops | bytes accessed | tf_op | source)
XLA Modules:
  0.0 248.2 jit_solution(4559328346790263488)
XLA Ops:
  10.5 34.2 %all-gather.2.cloned.1.call-done = bf16[512,2048]{1,0:T(8,128)(2,1)} async-done(((bf16[256,2048]{1,0:T(8,128)(2,1)}), bf16[512,2048]{1,0:T(8,128)(2,1)}) %all-gather.2.cloned.1.call-update) | async-done | bytes 2097168 | tf_op jit(solution)/shard_map/all_gather | solution.py:85
  44.7 2.2 fusion
  47.0 4.7 %convolution_convert_fusion = bf16[512,1024]{1,0:T(8,128)(2,1)S(1)} fusion(bf16[2048,1024]{1,0:T(8,128)(2,1)} %param.16, bf16[512,2048]{1,0:T(8,128)(2,1)S(1)} %copy-done.8, f32[2048]{0:T(1024)S(1)} %convert_element_type.85, f32[512]{0:T(512)S(1)} %add_rsqrt_fusion), kind=kOutput, calls=%fused_computation.44 | convolution fusion | flops 2152202240 | bytes 7350272 | tf_op jit(solution)/shard_map/dot_general | solution.py:29
  56.0 4.5 %collective-permute-start.6 = (bf16[8,512]{1,0:T(8,128)(2,1)S(1)}, bf16[8,512]{1,0:T(8,128)(2,1)S(1)}, u32[]{:S(2)}, u32[]{:S(2)}) collective-permute-start(bf16[8,512]{1,0:T(8,128)(2,1)S(1)} %get-tuple-element.24), channel_id=1, source_target_pairs={{0,2},{2,4},{4,6},{6,8},{8,10},{10,12},{12,14},{14,16},{16,18},{18... | collective-permute-start | bytes 24584 | tf_op jit(solution)/shard_map/ppermute | solution.py:16
  62.1 2.6 %fusion.71 = (f32[512,1024]{1,0:T(8,128)}, bf16[512,1024]{1,0:T(8,128)(2,1)}) fusion(f32[516,1024]{1,0:T(8,128)S(1)} %maximum_convert_fusion, f32[1024]{0:T(1024)S(1)} %bitcast.154, f32[1024]{0:T(1024)S(1)} %bitcast.155, f32[1024]{0:T(1024)S(1)} %bitcast.153, f32[1024]{0:T(1024)S(1)} %bitcast.152), kind=kLoop, calls=%fused_computation.231 | loop fusion | flops 4718592 | bytes 11550720 | tf_op jit(solution)/shard_map/convert_element_type | solution.py:108
  64.7 2.8 %copy.33 = bf16[512,1024]{0,1:T(8,128)(2,1)} copy(bf16[512,1024]{1,0:T(8,128)(2,1)} %get-tuple-element.8) | data formatting | bytes 2097152 | tf_op jit(solution)/shard_map/convert_element_type | solution.py:107
  67.5 2.4 fusion.96
  69.9 1.8 copy.35
  71.7 4.2 %fusion.74 = (f32[512,2,1,1024]{0,3,2,1:T(8,128)}, f32[512,2,1,1024]{0,3,2,1:T(8,128)}) fusion(f32[512,2,2,1024]{0,3,2,1:T(8,128)S(1)} %bitcast.122), kind=kLoop, calls=%fused_computation.233 | loop fusion | bytes 16777216 | tf_op jit(solution)/shard_map/slice | solution.py:117
  75.9 5.4 %copy.72 = f32[512,2,1,1024]{3,0,1,2:T(8,128)} copy(f32[512,2,1,1024]{0,3,2,1:T(8,128)} %get-tuple-element.12) | data formatting | bytes 8388608
  81.3 5.4 %copy.73 = f32[512,2,1,1024]{3,0,1,2:T(8,128)} copy(f32[512,2,1,1024]{0,3,2,1:T(8,128)} %get-tuple-element.13) | data formatting | bytes 8388608
  86.7 7.3 %fusion.3 = (f32[512,2,1024]{2,0,1:T(8,128)S(1)}, f32[512,2,1024]{2,0,1:T(8,128)S(1)}) fusion(f32[512,2,1,1024]{3,0,1,2:T(8,128)} %copy.73, f32[512,1024]{1,0:T(8,128)} %get-tuple-element.7, f32[512,2]{0,1:T(2,128)S(1)} %bitcast.158, f32[2,1024]{1,0:T(2,128)S(1)} %compare_select_fusion, f32[512,2,1,1024]{3,0,1,2:T(8,128)} %copy.72, ...), kind=kLoop, calls=%fused_computation.8 | loop fusion | flops 13631488 | bytes 18890752 | tf_op jit(solution)/shard_map/mul | solution.py:127
  94.0 3.3 %fusion.75 = (f32[512,1,1024]{2,0,1:T(8,128)}, f32[512,1,1024]{2,0,1:T(8,128)S(1)}, f32[512,1,1024]{2,0,1:T(8,128)}, f32[512,1,1024]{2,0,1:T(8,128)}) fusion(f32[512,2,1024]{2,0,1:T(8,128)S(1)} %get-tuple-element.6, f32[512,2,1024]{2,0,1:T(8,128)S(1)} %get-tuple-element.5), kind=kLoop, calls=%fused_computation.234 | loop fusion | bytes 16777216 | tf_op jit(solution)/shard_map/slice | solution.py:128
  99.2 3.6 %fusion.73 = (f32[32,16,1024]{2,0,1:T(8,128)S(1)}, f32[32,16,1024]{2,0,1:T(8,128)}, f32[32,16,1024]{2,0,1:T(8,128)}) fusion(f32[32,16,1024]{2,1,0:T(8,128)S(1)} %bitcast.124, f32[32,16,1024]{2,0,1:T(8,128)S(1)} %fusion.20, f32[32,1024]{1,0:T(8,128)S(1)} %slice_bitcast_fusion.2), kind=kLoop, calls=%fused_computation.232 | loop fusion | flops 1048576 | bytes 10616832 | tf_op jit(solution)/shard_map/exp | solution.py:48
  102.9 3.0 %copy.46 = f32[32,16,1024]{2,1,0:T(8,128)S(1)} copy(f32[32,16,1024]{2,0,1:T(8,128)} %get-tuple-element.10) | data formatting | bytes 4194304 | tf_op jit(solution)/shard_map/add | solution.py:40
  105.9 12.3 %multiply_reduce_fusion = f32[32,1024,16]{1,2,0:T(8,128)S(1)} fusion(f32[32,1024,16]{1,2,0:T(8,128)S(1)} %bitcast.139, f32[32,16,1024]{2,1,0:T(8,128)S(1)} %copy.46, pred[16,16]{1,0:T(8,128)(4,1)S(1)} %iota_compare_fusion), kind=kLoop, calls=%fused_computation | loop fusion | flops 41418752 | bytes 6291712
  120.9 4.3 %fusion.95 = (f32[32,16,1024]{2,0,1:T(8,128)S(1)}, f32[32,16,1024]{2,0,1:T(8,128)}) fusion(f32[32,16,1024]{2,1,0:T(8,128)} %bitcast.125), kind=kOutput, calls=%fused_computation.254 | output fusion | flops 7864320 | bytes 6291456 | tf_op jit(solution)/shard_map/jit(cumsum)/reduce_window_sum | solution.py:37
  125.3 3.0 %copy.39 = f32[32,16,1024]{2,1,0:T(8,128)S(1)} copy(f32[32,16,1024]{2,0,1:T(8,128)} %get-tuple-element.97) | data formatting | bytes 4194304 | tf_op jit(solution)/shard_map/jit(cumsum)/reduce_window_sum | solution.py:37
  128.3 12.1 %multiply_reduce_fusion.1 = f32[32,1024,16]{1,2,0:T(8,128)S(1)} fusion(f32[32,1024,16]{1,2,0:T(8,128)S(1)} %bitcast.138, f32[32,16,1024]{2,1,0:T(8,128)S(1)} %copy.39, pred[16,16]{1,0:T(8,128)(4,1)S(1)} %iota_compare_fusion.1), kind=kLoop, calls=%fused_computation.1 | loop fusion | flops 41418752 | bytes 6291712
  142.5 4.1 %copy.44 = f32[32,16,1024]{2,1,0:T(8,128)} copy(f32[32,16,1024]{2,0,1:T(8,128)} %get-tuple-element.11) | data formatting | bytes 4194304 | tf_op jit(solution)/shard_map/sub | solution.py:40
  148.3 3.7 %multiply_add_fusion = f32[32,16,1024]{2,0,1:T(8,128)S(1)} fusion(f32[32,1024]{1,0:T(8,128)S(1)} %concatenate.134, f32[32,1024,16]{1,2,0:T(8,128)} %copy-done.2, f32[32,16,1024]{2,0,1:T(8,128)} %get-tuple-element.10), kind=kLoop, calls=%fused_computation.39 | loop fusion | flops 1048576 | bytes 6422528 | tf_op jit(solution)/shard_map/add | solution.py:62
  154.9 2.8 %bitcast_multiply_fusion.2 = f32[512,1024]{1,0:T(8,128)S(1)} fusion(f32[32,16,1024]{2,1,0:T(8,128)} %copy.44, f32[32,1024]{1,0:T(8,128)S(1)} %concatenate.129, f32[512,2,1024]{2,0,1:T(8,128)} %copy-done.1), kind=kLoop, calls=%fused_computation.32 | loop fusion | flops 1048576 | bytes 6422528 | tf_op jit(solution)/shard_map/mul | solution.py:61
  159.9 3.7 %broadcast_multiply_fusion = (f32[32,16,1024]{2,0,1:T(8,128)S(1)}, f32[32,16,1024]{2,0,1:T(8,128)S(1)}) fusion(f32[32,1024]{1,0:T(8,128)S(1)} %concatenate.124, f32[32,16,1024]{2,0,1:T(8,128)} %get-tuple-element.97, f32[32,1024]{1,0:T(8,128)S(1)} %concatenate.119, f32[32,1024,16]{1,2,0:T(8,128)} %copy-done.3), kind=kLoop, calls=%fused_computation.62 | loop fusion | flops 1572864 | bytes 8650752 | tf_op jit(solution)/shard_map/mul | solution.py:61
  166.2 2.4 collective-permute-start.2
  169.5 2.4 collective-permute-start.3
  172.2 1.9 collective-permute-done.3
  174.2 3.6 %collective-permute-start.4 = (f32[4,4,1024]{2,1,0:T(4,128)S(1)}, f32[4,4,1024]{2,1,0:T(4,128)S(1)}, u32[]{:S(2)}, u32[]{:S(2)}) collective-permute-start(f32[4,4,1024]{2,1,0:T(4,128)S(1)} %maximum_select_fusion.2), channel_id=1, source_target_pairs={{0,8},{2,10},{4,12},{6,14},{8,0},{10,2},{12,4},{14,6},{16,24},{18,... | collective-permute-start | bytes 196616 | tf_op jit(solution)/shard_map/ppermute | solution.py:137
  180.0 3.0 %collective-permute-start.5 = (f32[8,4,1024]{2,1,0:T(4,128)S(1)}, f32[8,4,1024]{2,1,0:T(4,128)S(1)}, u32[]{:S(2)}, u32[]{:S(2)}) collective-permute-start(f32[8,4,1024]{2,1,0:T(4,128)S(1)} %maximum_select_fusion.1), channel_id=1, source_target_pairs={{0,16},{2,18},{4,20},{6,22},{8,24},{10,26},{12,28},{14,30},{16,0},... | collective-permute-start | bytes 393224 | tf_op jit(solution)/shard_map/ppermute | solution.py:137
  183.2 2.8 %collective-permute-done.5 = f32[8,4,1024]{2,1,0:T(4,128)S(1)} collective-permute-done((f32[8,4,1024]{2,1,0:T(4,128)S(1)}, f32[8,4,1024]{2,1,0:T(4,128)S(1)}, u32[]{:S(2)}, u32[]{:S(2)}) %collective-permute-start.5) | collective-permute-done | bytes 131104 | tf_op jit(solution)/shard_map/ppermute | solution.py:137
  189.5 13.7 %fusion.28 = f32[512,2048]{1,0:T(8,128)} fusion(bf16[1024,2048]{1,0:T(8,128)(2,1)} %param.26, f32[512,1024]{1,0:T(8,128)} %copy-done.4, f32[512,1024]{1,0:T(8,128)} %bitcast.133, f32[512,1024]{1,0:T(8,128)} %bitcast.137, f32[512,1024]{1,0:T(8,128)} %bitcast.135, bf16[2048,1024]{1,0:T(8,128)(2,1)} %param.17, f32[1024]{0:T(1024)S(1)} %bitcast.157, ...), kind=kOutput, calls=%fused_computation.63 | convolution fusion | flops 4308074496 | bytes 23087104 | tf_op jit(solution)/shard_map/dot_general | solution.py:29
  203.2 4.8 %add_convert_fusion = bf16[512,2048]{1,0:T(8,128)(2,1)} fusion(f32[512,2048]{1,0:T(8,128)} %fusion.28, bf16[512,512]{0,1:T(8,128)(2,1)S(1)} %fusion.27, bf16[512,2048]{1,0:T(8,128)(2,1)S(1)} %copy-done), kind=kOutput, calls=%fused_computation.12 | convolution fusion | flops 1075838976 | bytes 8912896 | tf_op jit(solution)/shard_map/dot_general | solution.py:29
  208.1 33.0 %reduce-scatter.2.cloned.1.call-done = bf16[256,2048]{1,0:T(8,128)(2,1)} async-done(((bf16[512,2048]{1,0:T(8,128)(2,1)}), bf16[256,2048]{1,0:T(8,128)(2,1)}) %reduce-scatter.2.cloned.1.call-update) | async-done | bytes 1048592 | tf_op jit(solution)/shard_map/reduce_scatter | solution.py:190
  (338 shorter events, 31.6 us)
Async XLA Ops:
  6.5 196.7 %copy-start = (bf16[512,2048]{1,0:T(8,128)(2,1)S(1)}, bf16[512,2048]{1,0:T(8,128)(2,1)}, u32[]{:S(2)}) copy-start(bf16[512,2048]{1,0:T(8,128)(2,1)} %param.27) | copy-start | bytes 6291460
  6.5 3.9 %copy-start.15 = (f32[2,512]{1,0:T(2,128)S(1)}, f32[2,512]{1,0:T(2,128)}, u32[]{:S(2)}) copy-start(f32[2,512]{1,0:T(2,128)} %param.22) | copy-start | bytes 12292
  6.5 3.9 %copy-start.14 = (f32[2,1024]{1,0:T(2,128)S(1)}, f32[2,1024]{1,0:T(2,128)}, u32[]{:S(2)}) copy-start(f32[2,1024]{1,0:T(2,128)} %param.21) | copy-start | bytes 24580
  6.5 4.0 %copy-start.13 = (bf16[4,1024]{1,0:T(4,128)(2,1)S(1)}, bf16[4,1024]{1,0:T(4,128)(2,1)}, u32[]{:S(2)}) copy-start(bf16[4,1024]{1,0:T(4,128)(2,1)} %param.19) | copy-start | bytes 24580
  6.5 38.2 %all-gather.2.cloned.1.call-start = ((), (), s32[]{:S(2)}) async-start(), calls=%async_computation.1 | async-start | bytes 3145728 | tf_op jit(solution)/shard_map/all_gather | solution.py:85
  7.3 233.9 %reduce-scatter.2.cloned.1.call-start = ((), (), s32[]{:S(2)}) async-start(), calls=%async_computation.2 | async-start | bytes 3145728 | tf_op jit(solution)/shard_map/reduce_scatter | solution.py:190
  44.7 2.2 copy-start.8
  47.0 7.6 %copy-start.17 = (bf16[2048,512]{1,0:T(8,128)(2,1)S(1)}, bf16[2048,512]{1,0:T(8,128)(2,1)}, u32[]{:S(2)}) copy-start(bf16[2048,512]{1,0:T(8,128)(2,1)} %param.18) | copy-start | bytes 6291460
  51.8 10.0 %collective-permute-start = (bf16[2,1024]{1,0:T(2,128)(2,1)S(1)}, bf16[2,1024]{1,0:T(2,128)(2,1)S(1)}, u32[]{:S(2)}, u32[]{:S(2)}) collective-permute-start(bf16[2,1024]{1,0:T(2,128)(2,1)S(1)} %get-tuple-element.22), channel_id=1, source_target_pairs={{0,2},{2,4},{4,6},{6,8},{8,10},{10,12},{12,14},{14,16},{16,18},{18... | collective-permute-start | bytes 12296 | tf_op jit(solution)/shard_map/ppermute | solution.py:16
  53.3 8.4 %collective-permute-start.1 = (bf16[2,1024]{1,0:T(2,128)(2,1)S(1)}, bf16[2,1024]{1,0:T(2,128)(2,1)S(1)}, u32[]{:S(2)}, u32[]{:S(2)}) collective-permute-start(bf16[2,1024]{1,0:T(2,128)(2,1)S(1)} %get-tuple-element.23), channel_id=1, source_target_pairs={{2,0},{4,2},{6,4},{8,6},{10,8},{12,10},{14,12},{16,14},{18,16},{20... | collective-permute-start | bytes 12296 | tf_op jit(solution)/shard_map/ppermute | solution.py:19
  55.9 6.1 %copy-start.11 = (bf16[512,512]{1,0:T(8,128)(2,1)}, bf16[512,512]{1,0:T(8,128)(2,1)S(1)}, u32[]{:S(2)}) copy-start(bf16[512,512]{1,0:T(8,128)(2,1)S(1)} %convolution_convert_fusion.2) | copy-start | bytes 1572868
  56.0 112.7 %collective-permute-start.6 = (bf16[8,512]{1,0:T(8,128)(2,1)S(1)}, bf16[8,512]{1,0:T(8,128)(2,1)S(1)}, u32[]{:S(2)}, u32[]{:S(2)}) collective-permute-start(bf16[8,512]{1,0:T(8,128)(2,1)S(1)} %get-tuple-element.24), channel_id=1, source_target_pairs={{0,2},{2,4},{4,6},{6,8},{8,10},{10,12},{12,14},{14,16},{16,18},{18... | collective-permute-start | bytes 24584 | tf_op jit(solution)/shard_map/ppermute | solution.py:16
  60.4 108.2 %collective-permute-start.7 = (bf16[8,512]{1,0:T(8,128)(2,1)S(1)}, bf16[8,512]{1,0:T(8,128)(2,1)S(1)}, u32[]{:S(2)}, u32[]{:S(2)}) collective-permute-start(bf16[8,512]{1,0:T(8,128)(2,1)S(1)} %get-tuple-element.25), channel_id=1, source_target_pairs={{2,0},{4,2},{6,4},{8,6},{10,8},{12,10},{14,12},{16,14},{18,16},{20... | collective-permute-start | bytes 24584 | tf_op jit(solution)/shard_map/ppermute | solution.py:19
  81.3 5.4 %copy-start.16 = (f32[2,512]{1,0:T(2,128)S(1)}, f32[2,512]{1,0:T(2,128)}, u32[]{:S(2)}) copy-start(f32[2,512]{1,0:T(2,128)} %param.23) | copy-start | bytes 12292
  94.0 3.9 %copy-start.1 = (f32[512,2,1024]{2,0,1:T(8,128)}, f32[512,2,1024]{2,0,1:T(8,128)S(1)}, u32[]{:S(2)}) copy-start(f32[512,2,1024]{2,0,1:T(8,128)S(1)} %get-tuple-element.6) | copy-start | bytes 12582916
  102.9 3.0 %copy-start.10 = (f32[512,1,1024]{2,0,1:T(8,128)S(1)}, f32[512,1,1024]{2,0,1:T(8,128)}, u32[]{:S(2)}) copy-start(f32[512,1,1024]{2,0,1:T(8,128)} %get-tuple-element.98) | copy-start | bytes 6291460
  118.2 1.3 copy-start.2
  125.3 3.0 %copy-start.9 = (f32[512,1,1024]{2,0,1:T(8,128)S(1)}, f32[512,1,1024]{2,0,1:T(8,128)}, u32[]{:S(2)}) copy-start(f32[512,1,1024]{2,0,1:T(8,128)} %get-tuple-element.99) | copy-start | bytes 6291460
  140.4 1.3 copy-start.3
  153.2 1.4 copy-start.5
  157.7 1.4 copy-start.4
  164.8 1.3 copy-start.6
  164.9 3.8 %copy-start.12 = (bf16[512,512]{1,0:T(8,128)(2,1)S(1)}, bf16[512,512]{1,0:T(8,128)(2,1)}, u32[]{:S(2)}) copy-start(bf16[512,512]{1,0:T(8,128)(2,1)} %copy-done.11) | copy-start | bytes 1572868
  166.2 2.8 %copy-start.7 = (f32[32,16,1024]{2,1,0:T(8,128)}, f32[32,16,1024]{2,1,0:T(8,128)S(1)}, u32[]{:S(2)}) copy-start(f32[32,16,1024]{2,1,0:T(8,128)S(1)} %copy.41) | copy-start | bytes 6291460
  166.2 3.3 %collective-permute-start.2 = (f32[1,4,1024]{2,1,0:T(4,128)S(1)}, f32[1,4,1024]{2,1,0:T(4,128)S(1)}, u32[]{:S(2)}, u32[]{:S(2)}) collective-permute-start(f32[1,4,1024]{2,1,0:T(4,128)S(1)} %maximum_bitcast_fusion), channel_id=1, source_target_pairs={{0,2},{2,0},{4,6},{6,4},{8,10},{10,8},{12,14},{14,12},{16,18},{18,... | collective-permute-start | bytes 49160 | tf_op jit(solution)/shard_map/ppermute | solution.py:137
  169.5 8.2 %copy-start.18 = (bf16[4,128,128]{2,1,0:T(8,128)(2,1)S(1)}, bf16[4,128,128]{2,1,0:T(8,128)(2,1)}, u32[]{:S(2)}) copy-start(bf16[4,128,128]{2,1,0:T(8,128)(2,1)} %param.24) | copy-start | bytes 393220
  169.5 4.6 %collective-permute-start.3 = (f32[2,4,1024]{2,1,0:T(4,128)S(1)}, f32[2,4,1024]{2,1,0:T(4,128)S(1)}, u32[]{:S(2)}, u32[]{:S(2)}) collective-permute-start(f32[2,4,1024]{2,1,0:T(4,128)S(1)} %maximum_select_fusion.3), channel_id=1, source_target_pairs={{0,4},{2,6},{4,0},{6,2},{8,12},{10,14},{12,8},{14,10},{16,20},{18,... | collective-permute-start | bytes 98312 | tf_op jit(solution)/shard_map/ppermute | solution.py:137
  174.2 5.8 %collective-permute-start.4 = (f32[4,4,1024]{2,1,0:T(4,128)S(1)}, f32[4,4,1024]{2,1,0:T(4,128)S(1)}, u32[]{:S(2)}, u32[]{:S(2)}) collective-permute-start(f32[4,4,1024]{2,1,0:T(4,128)S(1)} %maximum_select_fusion.2), channel_id=1, source_target_pairs={{0,8},{2,10},{4,12},{6,14},{8,0},{10,2},{12,4},{14,6},{16,24},{18,... | collective-permute-start | bytes 196616 | tf_op jit(solution)/shard_map/ppermute | solution.py:137
  180.0 6.0 %collective-permute-start.5 = (f32[8,4,1024]{2,1,0:T(4,128)S(1)}, f32[8,4,1024]{2,1,0:T(4,128)S(1)}, u32[]{:S(2)}, u32[]{:S(2)}) collective-permute-start(f32[8,4,1024]{2,1,0:T(4,128)S(1)} %maximum_select_fusion.1), channel_id=1, source_target_pairs={{0,16},{2,18},{4,20},{6,22},{8,24},{10,26},{12,28},{14,30},{16,0},... | collective-permute-start | bytes 393224 | tf_op jit(solution)/shard_map/ppermute | solution.py:137
Sparse Core Ops, SparseCore 0:
  8.9 35.8 all-gather.1
  208.2 32.8 reduce-scatter.1
